TPU v7x, 32 devices: a whole 2x2x4 slice. The times are simulated.
32 devices in a mesh: sp: 16 (over z, y, x), tp: 2 (over core).
Axes of the slice: x: 2, y: 2, z: 4, core: 2. Of those that a mesh axis runs over, the one named last changes fastest.
Arguments:
- tokens: bfloat16 [2048, 2048], P(('sp', 'tp')), may hold values from -6 to 6
- input_norm_gain: float32 [2048], replicated, may hold values from 0.1 to 1.9
- differential_query: bfloat16 [2048, 1024], P(None, 'tp'), may hold values from -0.176776695 to 0.176776695, as said below
- differential_key: bfloat16 [2048, 1024], P(None, 'tp'), may hold values from -0.176776695 to 0.176776695, as said below
- differential_value: bfloat16 [2048, 1024], P(None, 'tp'), may hold values from -0.125 to 0.125
- query_norm_gain: float32 [64], replicated, may hold values from 1.15 to 5
- key_norm_gain: float32 [64], replicated, may hold values from 1.15 to 5
- second_map_weight: float32 [8], P('tp'), may hold values from 0.3 to 0.8
- differential_norm_gain: float32 [128], replicated, may hold values from 0.1 to 1.9
- linear_query: bfloat16 [2048, 512], P(None, 'tp'), may hold values from -0.125 to 0.125
- linear_key: bfloat16 [2048, 512], P(None, 'tp'), may hold values from -0.125 to 0.125
- linear_value: bfloat16 [2048, 1024], P(None, 'tp'), may hold values from -0.125 to 0.125
- linear_output_gate: bfloat16 [2048, 1024], P(None, 'tp'), may hold values from -0.125 to 0.125
- forget_down_factor: bfloat16 [2048, 32], replicated, may hold values from -0.125 to 0.125
- forget_up_factor: bfloat16 [32, 512], P(None, 'tp'), may hold values from -2.109375 to 2.109375
- forget_bias: float32 [512], P('tp'), may hold values from -0.5 to 10
- extra_shrinkage_exponent: float32 [2048, 8], P('sp', 'tp'), may hold values from -1.5 to 0
- linear_norm_gain: float32 [128], replicated, may hold values from 0.1 to 1.9
- differential_output_rows: bfloat16 [1024, 2048], P('tp'), may hold values from -0.125 to 0.125
- linear_output_rows: bfloat16 [1024, 2048], P('tp'), may hold values from -0.125 to 0.125
Outputs:
- layer_out: bfloat16 [2048, 2048], P(('sp', 'tp'))
Inputs may be any that keep to these rules, and one draw needn't show every extreme that they name: `differential_query`: independent entries of scale one over sqrt(2048). `differential_key`: entries of scale one over sqrt(2048).
All inputs are finite; a program needn't handle non-finite values.
Results may differ from a plain program's by a relative error of at most 0.015.
Values may be sent and summed in bfloat16 or wider, within the bound.
A program may use at most 64 MiB of HBM per device.

v0:
```python
from functools import partial
import jax
import jax.numpy as jnp
from jax import lax
from jax.sharding import PartitionSpec as P

HEAD = 64
VDIM = 128
RECURRENT_DIM = 64
GLA_DV = 128
BLOCK = 64
RMS_EPS = 1e-06
SOFTMAX_DIVISOR = 16.0
OUT_SCALE = 0.8
NEG_LARGE = -1e30
HIGHEST = lax.Precision.HIGHEST


def partner(block, axis, apart):
    count = lax.axis_size(axis)
    route = []
    for low in range(count):
        high = low | 1 << apart
        if high != low and high < count:
            route += [(low, high), (high, low)]
    return lax.ppermute(block, axis, route)


def prefix(shard, axis, combine, identity):
    devices, position = (lax.axis_size(axis), lax.axis_index(axis))
    everything = jax.tree.map(lambda part: lax.all_gather(part, axis), shard)
    start = jax.tree.map(
        lambda part, zero: jnp.broadcast_to(jnp.asarray(zero, part.dtype), part.shape),
        shard,
        identity,
    )

    def turn(k, before):
        reached = k < position
        new = combine(before, jax.tree.map(lambda part: part[k], everything))
        return jax.tree.map(lambda a, b: jnp.where(reached, a, b), new, before)

    return lax.fori_loop(0, devices, turn, start)


def rms_scale(values, scale_gain):
    mean_sq = jnp.mean(values * values, axis=-1, keepdims=True)
    return values * lax.rsqrt(mean_sq + RMS_EPS) * scale_gain


def block_length(total_rows, shard_rows):
    best = shard_rows
    shard_total = total_rows // shard_rows
    for multiple in range(1, shard_total + 1):
        if shard_total % multiple == 0 and shard_rows * multiple <= 2048:
            best = shard_rows * multiple
    return best


def combine_chain(earlier, later):
    return (earlier[0] * later[0], earlier[1] * later[0][..., None] + later[1])


def keep_carry(carry_now):
    return carry_now


def attend_span(query_set, query_pos, keys_here, values_here, key_pos, carry_now):
    row_peaks, totals, numerators = carry_now
    query_rows = query_set.shape[0]
    group_count = query_set.shape[1]
    attn_heads = group_count // 2
    span_rows = keys_here.shape[0]
    scores = jnp.einsum(
        "tgd,kgd->gtk", query_set, keys_here, preferred_element_type=jnp.float32
    ) * HEAD ** (-0.5)
    causal = key_pos[None, :] <= query_pos[:, None]
    scores = jnp.where(causal[None], scores, NEG_LARGE)
    new_peaks = jnp.maximum(row_peaks, jnp.max(scores, axis=-1))
    weights = jnp.where(causal[None], jnp.exp(scores - new_peaks[..., None]), 0.0)
    factor = jnp.exp(row_peaks - new_peaks)
    totals = totals * factor + jnp.sum(weights, axis=-1)
    rounded = weights.astype(jnp.bfloat16).reshape(attn_heads, 2, query_rows, span_rows)
    contrib = jnp.einsum(
        "hmtk,khv->hmtv", rounded, values_here, preferred_element_type=jnp.float32
    ).reshape(group_count, query_rows, VDIM)
    return (new_peaks, totals, numerators * factor[..., None] + contrib)


def per_device(
    tokens,
    input_norm_gain,
    differential_query,
    differential_key,
    differential_value,
    query_norm_gain,
    key_norm_gain,
    second_map_weight,
    differential_norm_gain,
    linear_query,
    linear_key,
    linear_value,
    linear_output_gate,
    forget_down_factor,
    forget_up_factor,
    forget_bias,
    extra_shrinkage_exponent,
    linear_norm_gain,
    differential_output_rows,
    linear_output_rows,
):
    sp_size = lax.axis_size("sp")
    sp_index = lax.axis_index("sp")
    attn_heads = second_map_weight.shape[0]
    linear_head_list = extra_shrinkage_exponent.shape[1]
    normed = rms_scale(tokens.astype(jnp.float32), input_norm_gain).astype(jnp.bfloat16)
    parts_list = [
        differential_query,
        differential_key,
        differential_value,
        linear_query,
        linear_key,
        linear_value,
        linear_output_gate,
        forget_down_factor,
    ]
    packed = jnp.concatenate(parts_list, axis=1)
    bounds = [0]
    for matrix in parts_list:
        bounds.append(bounds[-1] + matrix.shape[1])
    projected = jnp.dot(
        lax.all_gather(normed, "tp", axis=0, tiled=True), packed, preferred_element_type=jnp.float32
    ).astype(jnp.bfloat16)
    row_count = projected.shape[0]
    half_rows = row_count // 2
    bit_count = sp_size.bit_length() - 1

    def section(column_set):
        return projected[:, bounds[column_set] : bounds[column_set + 1]]

    group_count = 2 * attn_heads
    query_norm = rms_scale(
        section(0).astype(jnp.float32).reshape(row_count, group_count, HEAD), query_norm_gain
    ).astype(jnp.bfloat16)
    key_norm = rms_scale(
        section(1).astype(jnp.float32).reshape(row_count, group_count, HEAD), key_norm_gain
    ).astype(jnp.bfloat16)
    key_flat = key_norm.reshape(row_count, group_count * HEAD)
    value_flat = section(2)
    far_queries = query_norm[half_rows:].reshape(half_rows, group_count * HEAD)
    for bit in range(bit_count):
        far_queries = partner(far_queries, "sp", bit)
    mirror_index = sp_size - 1 - sp_index
    own_pos = sp_index * row_count + jnp.arange(half_rows, dtype=jnp.int32)
    far_pos = mirror_index * row_count + half_rows + jnp.arange(half_rows, dtype=jnp.int32)
    query_sets = [
        (query_norm[:half_rows], own_pos),
        (far_queries.reshape(half_rows, group_count, HEAD), far_pos),
    ]
    fold_start = tuple(
        (
            (
                jnp.full((group_count, query_set.shape[0]), NEG_LARGE, jnp.float32),
                jnp.zeros((group_count, query_set.shape[0]), jnp.float32),
                jnp.zeros((group_count, query_set.shape[0], VDIM), jnp.float32),
            )
            for query_set, query_pos in query_sets
        )
    )
    key_rows = lax.all_gather(key_flat, "sp", axis=0, tiled=True)
    value_rows = lax.all_gather(value_flat, "sp", axis=0, tiled=True)
    piece_rows = key_rows.shape[0]
    span_rows = block_length(piece_rows, row_count)

    def attend(span_index, carries):
        row_start = span_index * span_rows
        keys_here = lax.dynamic_slice_in_dim(
            key_rows, span_index * span_rows, span_rows, 0
        ).reshape(span_rows, group_count, HEAD)
        values_here = lax.dynamic_slice_in_dim(
            value_rows, span_index * span_rows, span_rows, 0
        ).reshape(span_rows, attn_heads, VDIM)
        key_pos = row_start + jnp.arange(span_rows, dtype=jnp.int32)
        results = []
        for (query_set, query_pos), carry_in in zip(query_sets, carries):
            work = partial(attend_span, query_set, query_pos, keys_here, values_here, key_pos)
            results.append(lax.cond(row_start <= jnp.max(query_pos), work, keep_carry, carry_in))
        return tuple(results)

    folded = lax.fori_loop(0, piece_rows // span_rows, attend, fold_start)

    def finish(carry_set):
        row_peaks, totals, numerators = carry_set
        set_rows = totals.shape[1]
        maps_out = (numerators / totals[..., None]).reshape(attn_heads, 2, set_rows, VDIM)
        attn_mix = maps_out[:, 0] - second_map_weight[:, None, None] * maps_out[:, 1]
        return (
            (rms_scale(attn_mix, differential_norm_gain) * OUT_SCALE)
            .transpose(1, 0, 2)
            .reshape(set_rows, attn_heads * VDIM)
            .astype(jnp.bfloat16)
        )

    own_rows = finish(folded[0])
    far_rows = finish(folded[1])
    for bit in range(bit_count):
        far_rows = partner(far_rows, "sp", bit)
    attn_out = jnp.concatenate([own_rows, far_rows], axis=0)
    chain_queries = section(3).astype(jnp.float32).reshape(
        row_count, linear_head_list, RECURRENT_DIM
    ) * RECURRENT_DIM ** (-0.5)
    chain_keys = section(4).astype(jnp.float32).reshape(row_count, linear_head_list, RECURRENT_DIM)
    chain_values = section(5).astype(jnp.float32).reshape(row_count, linear_head_list, GLA_DV)
    gated = jax.nn.silu(section(6).astype(jnp.float32)).reshape(row_count, linear_head_list, GLA_DV)
    sigmoid_preactivation = (
        jnp.dot(section(7), forget_up_factor, preferred_element_type=jnp.float32) + forget_bias
    )
    shrinkage_exponent = (
        jax.nn.log_sigmoid(sigmoid_preactivation).reshape(
            row_count, linear_head_list, RECURRENT_DIM
        )
        / SOFTMAX_DIVISOR
        + extra_shrinkage_exponent[:, :, None]
    )
    block_total = row_count // BLOCK

    def blockify(array):
        return array.reshape(block_total, BLOCK, linear_head_list, array.shape[-1])

    causal_block = jnp.arange(BLOCK)[:, None] >= jnp.arange(BLOCK)[None, :]

    def chain_block(carry, inputs):
        carried, log_total = carry
        query_block, key_block, value_block, decay_block = inputs
        log_cum = jnp.cumsum(decay_block, axis=0)
        log_last = log_cum[-1]
        query_decayed = query_block * jnp.exp(log_cum)
        key_inverse = key_block * jnp.exp(-log_cum)
        inner_scores = jnp.einsum("thd,shd->hts", query_decayed, key_inverse, precision=HIGHEST)
        inner_scores = jnp.where(causal_block[None], inner_scores, 0.0)
        local_out = jnp.einsum("hts,she->the", inner_scores, value_block, precision=HIGHEST)
        local_out = local_out + jnp.einsum(
            "thd,hde->the", query_decayed, carried, precision=HIGHEST
        )
        key_end = key_block * jnp.exp(log_last[None] - log_cum)
        carried = carried * jnp.exp(log_last)[..., None] + jnp.einsum(
            "thd,the->hde", key_end, value_block, precision=HIGHEST
        )
        carried_query = query_decayed * jnp.exp(log_total)[None]
        return ((carried, log_total + log_last), (local_out, carried_query))

    chain_zero = (
        jnp.zeros((linear_head_list, RECURRENT_DIM, GLA_DV), jnp.float32),
        jnp.zeros((linear_head_list, RECURRENT_DIM), jnp.float32),
    )
    (own_state, log_total), (local_out, carried_query) = lax.scan(
        chain_block,
        chain_zero,
        (
            blockify(chain_queries),
            blockify(chain_keys),
            blockify(chain_values),
            blockify(shrinkage_exponent),
        ),
    )
    local_out = local_out.reshape(row_count, linear_head_list, GLA_DV)
    carried_query = carried_query.reshape(row_count, linear_head_list, RECURRENT_DIM)
    own_decay = jnp.exp(log_total)
    carried_in = prefix(
        (own_decay, own_state),
        "sp",
        combine_chain,
        (jnp.ones_like(own_decay), jnp.zeros_like(own_state)),
    )[1]
    chain_full = local_out + jnp.einsum(
        "thd,hde->the", carried_query, carried_in, precision=HIGHEST
    )
    chain_out = (
        (rms_scale(chain_full, linear_norm_gain) * gated)
        .reshape(row_count, linear_head_list * GLA_DV)
        .astype(jnp.bfloat16)
    )
    return lax.psum_scatter(
        (
            jnp.dot(attn_out, differential_output_rows, preferred_element_type=jnp.float32)
            + jnp.dot(chain_out, linear_output_rows, preferred_element_type=jnp.float32)
        ).astype(jnp.bfloat16),
        "tp",
        scatter_dimension=0,
        tiled=True,
    )


def solution(mesh):
    placed = (
        P(("sp", "tp"), None),
        P(),
        P(None, "tp"),
        P(None, "tp"),
        P(None, "tp"),
        P(),
        P(),
        P("tp"),
        P(),
        P(None, "tp"),
        P(None, "tp"),
        P(None, "tp"),
        P(None, "tp"),
        P(),
        P(None, "tp"),
        P("tp"),
        P("sp", "tp"),
        P(),
        P("tp", None),
        P("tp", None),
    )
    return jax.shard_map(
        per_device, mesh=mesh, in_specs=placed, out_specs=P(("sp", "tp"), None), check_vma=False
    )
```

profile of v0, /device:TPU:0, one launch (start us, length us, event | category | flops | bytes accessed | tf_op | source)
XLA Modules:
  0.0 273.5 jit_solution(2683229393621899004)
XLA Ops:
  6.6 3.3 %constant_dynamic-update-slice_fusion.7 = bf16[2048,3104]{1,0:T(8,128)(2,1)} fusion(bf16[2048,512]{1,0:T(8,128)(2,1)} %param.30), kind=kLoop, calls=%fused_computation.130 | loop fusion | bytes 4194304
  10.5 2.4 all_gather.21
  13.0 3.2 %constant_dynamic-update-slice_fusion.6 = bf16[2048,3104]{1,0:T(8,128)(2,1)} fusion(bf16[2048,3104]{1,0:T(8,128)(2,1)} %constant_dynamic-update-slice_fusion.7, bf16[2048,512]{1,0:T(8,128)(2,1)} %param.31), kind=kLoop, calls=%fused_computation.129 | loop fusion | bytes 4194304
  16.2 1.5 constant_dynamic-update-slice_fusion.5
  17.8 1.1 constant_dynamic-update-slice_fusion.4
  18.8 1.1 constant_dynamic-update-slice_fusion.3
  19.9 1.6 constant_dynamic-update-slice_fusion.2
  21.5 1.5 constant_dynamic-update-slice_fusion.1
  23.9 8.3 %convolution_convert_fusion = bf16[128,3104]{0,1:T(8,128)(2,1)S(1)} fusion(bf16[128,2048]{1,0:T(8,128)(2,1)S(1)} %all_gather.21, bf16[2048,3104]{1,0:T(8,128)(2,1)} %constant_dynamic-update-slice_fusion), kind=kOutput, calls=%fused_computation.68 | convolution fusion | flops 1627787264 | bytes 14032896 | tf_op jit(solution)/shard_map/dot_general | solution.py:131
  35.4 1.1 reshape.228
  36.5 1.2 copy.125
  38.7 1.1 div.64
  39.9 1.1 mul.296
  41.0 1.8 reshape.219
  43.7 10.5 %while.8 = (s32[]{:T(128)}, f32[4,64,128]{2,1,0:T(8,128)S(1)}, f32[4,64]{1,0:T(4,128)S(1)}, f32[2,64,4,128]{3,1,0,2:T(8,128)}, f32[2,64,4,64]{3,2,1,0:T(4,128)},...) while((s32[]{:T(128)}, f32[4,64,128]{2,1,0:T(8,128)S(1)}, ...), condition=%wide.region_17.18_spmd.clone, body=%wide.region_15.0_spmd.clone.sunk | while | flops 89412096 | bytes 2970753 | solution.py:256
  43.7 1.2 constant_dynamic-slice_fusion.3
  49.0 1.2 constant_dynamic-slice_fusion.3
  55.6 2.9 %collective-permute-start = (bf16[64,512]{1,0:T(8,128)(2,1)S(1)}, bf16[64,512]{1,0:T(8,128)(2,1)S(1)}, u32[]{:S(2)}, u32[]{:S(2)}) collective-permute-start(bf16[64,512]{1,0:T(8,128)(2,1)S(1)} %reshape.212), channel_id=1, source_target_pairs={{0,2},{2,0},{4,6},{6,4},{8,10},{10,8},{12,14},{14,12},{16,18},{18,... | collective-permute-start | bytes 196616 | tf_op jit(solution)/shard_map/ppermute | solution.py:26
  58.5 2.4 collective-permute-done
  60.9 1.9 collective-permute-start.1
  64.7 1.1 copy.129
  65.8 40.7 %all-gather.2 = f32[16,4,64]{2,1,0:T(4,128)S(1)} all-gather(f32[1,4,64]{2,1,0:T(4,128)S(1)} %exponential_bitcast_fusion), channel_id=2, replica_groups=mesh['sp'=16,'tp'=2] {'sp'}, dimensions={0}, use_global_device_ids=true | all-gather | bytes 17408 | tf_op jit(solution)/shard_map/all_gather | solution.py:31
  106.6 4.3 %collective-permute-done.2 = bf16[64,512]{1,0:T(8,128)(2,1)S(1)} collective-permute-done((bf16[64,512]{1,0:T(8,128)(2,1)S(1)}, bf16[64,512]{1,0:T(8,128)(2,1)S(1)}, u32[]{:S(2)}, u32[]{:S(2)}) %collective-permute-start.2) | collective-permute-done | bytes 65568 | tf_op jit(solution)/shard_map/ppermute | solution.py:26
  110.9 52.9 %all-gather.9.cloned.1.call-done = bf16[2048,512]{0,1:T(8,128)(2,1)} async-done(((bf16[128,512]{0,1:T(8,128)(2,1)}), bf16[2048,512]{0,1:T(8,128)(2,1)}) %all-gather.9.cloned.1.call-update) | async-done | bytes 2097168 | tf_op jit(solution)/shard_map/all_gather | solution.py:171
  163.8 5.5 %conditional.3 = (f32[8,64]{1,0:T(8,128)S(1)}, f32[8,64,128]{2,1,0:T(8,128)S(1)}) conditional(s32[]{:T(128)} %convert_element_type.81, (f32[8,64]{1,0:T(8,128)S(1)}, f32[8,64,128]{2,1,0:T(8,128)S(1)}) %tuple.49, (s32[2048]{0:T(1024)S(1)}, s32[64]{0:T(128)S(1)}, bf16[64,512]{1,0:T(8,128)(2,1)S(1)}, bf16[2048,8,64]{0,2,1:T(8,128)(2,1)}, ...), branch_computations={%region_10.0_spmd, %region_11.0_spmd} | conditional | flops 412353536 | bytes 26839340 | solution.py:187
  164.3 2.6 fusion.9
  166.9 1.3 fusion.10
  169.4 5.3 %conditional.2 = ((f32[8,64]{1,0:T(8,128)S(1)}, f32[8,64,128]{2,1,0:T(8,128)S(1)})) conditional(s32[]{:T(128)} %convert_element_type.71, (f32[8,64]{1,0:T(8,128)S(1)}, f32[8,64,128]{2,1,0:T(8,128)S(1)}) %tuple.49, (s32[2048]{0:T(1024)S(1)}, s32[64]{0:T(128)S(1)}, bf16[128,8,64]{2,0,1:T(8,128)(2,1)S(1)}, bf16[2048,8,64]{0,2,1:T(8,128)(2,1)}, ...), branch_computations={%region_4.5_spmd, %region_5.8_spmd} | conditional | flops 412353536 | bytes 26773812 | solution.py:187
  169.6 2.6 fusion.2
  172.2 1.3 fusion.3
  176.0 1.5 collective-permute-start.4
  177.4 47.9 %all-gather.11.cloned.1.call-done = f32[64,64,128]{2,1,0:T(8,128)} async-done(((f32[4,64,128]{2,1,0:T(8,128)}), f32[64,64,128]{2,1,0:T(8,128)}) %all-gather.11.cloned.1.call-update) | async-done | bytes 2097168 | tf_op jit(solution)/shard_map/all_gather | solution.py:31
  225.4 17.2 %while.9 = (s32[]{:T(128)}, f32[4,64,128]{2,1,0:T(8,128)S(1)}, s32[]{:T(128)}, f32[16,4,64]{2,1,0:T(4,128)S(1)}, f32[16,4,64,128]{3,2,1,0:T(8,128)}, /*index=5*/s32[]{:T(128)}, s32[]{:T(128)}) while((s32[]{:T(128)}, f32[4,64,128]{2,1,0:T(8,128)S(1)}, s32[]{:T(128)}, f32[16,4,64]{2,1,0:T(4,128)S(1)}, ...), condition=%wide.region_19.20_spmd.clone, body=%wide.region_18.19_spmd.clone.sunk | while | flops 131076 | bytes 396393 | solution.py:43
  226.5 1.0 fusion.107
  227.5 1.0 fusion.107
  228.6 1.0 fusion.107
  229.7 1.0 fusion.107
  230.8 1.0 fusion.107
  231.9 1.0 fusion.107
  242.7 1.7 multiply_reduce_fusion
  244.4 1.5 collective-permute-start.5
  245.9 2.8 %collective-permute-done.5 = bf16[64,512]{1,0:T(8,128)(2,1)S(1)} collective-permute-done((bf16[64,512]{1,0:T(8,128)(2,1)S(1)}, bf16[64,512]{1,0:T(8,128)(2,1)S(1)}, u32[]{:S(2)}, u32[]{:S(2)}) %collective-permute-start.5) | collective-permute-done | bytes 65568 | tf_op jit(solution)/shard_map/ppermute | solution.py:26
  248.7 1.5 collective-permute-start.6
  250.3 2.7 collective-permute-done.6
  253.0 1.8 collective-permute-start.7
  255.3 2.9 %collective-permute-done.7 = bf16[64,512]{1,0:T(8,128)(2,1)S(1)} collective-permute-done((bf16[64,512]{1,0:T(8,128)(2,1)S(1)}, bf16[64,512]{1,0:T(8,128)(2,1)S(1)}, u32[]{:S(2)}, u32[]{:S(2)}) %collective-permute-start.7) | collective-permute-done | bytes 65568 | tf_op jit(solution)/shard_map/ppermute | solution.py:26
  258.2 1.3 fusion.41
  259.4 7.6 %reduce-scatter.2.cloned.1.call-done = bf16[64,2048]{1,0:T(8,128)(2,1)} async-done(((bf16[128,2048]{1,0:T(8,128)(2,1)}), bf16[64,2048]{1,0:T(8,128)(2,1)}) %reduce-scatter.2.cloned.1.call-update) | async-done | bytes 262160 | tf_op jit(solution)/shard_map/reduce_scatter | solution.py:283
  (168 shorter events, 31.6 us)
Async XLA Ops:
  6.5 248.2 %copy-start = (bf16[512,2048]{1,0:T(8,128)(2,1)S(1)}, bf16[512,2048]{1,0:T(8,128)(2,1)}, u32[]{:S(2)}) copy-start(bf16[512,2048]{1,0:T(8,128)(2,1)} %param.47) | copy-start | bytes 6291460
  6.5 3.4 %copy-start.12 = (bf16[2048,32]{0,1:T(8,128)(2,1)S(1)}, bf16[2048,32]{0,1:T(8,128)(2,1)}, u32[]{:S(2)}) copy-start(bf16[2048,32]{0,1:T(8,128)(2,1)} %param.41) | copy-start | bytes 393220
  6.5 3.7 %copy-start.8 = (bf16[64,2048]{1,0:T(8,128)(2,1)S(1)}, bf16[64,2048]{1,0:T(8,128)(2,1)}, u32[]{:S(2)}) copy-start(bf16[64,2048]{1,0:T(8,128)(2,1)} %param.28) | copy-start | bytes 786436
  6.5 3.9 %copy-start.13 = (f32[2048]{0:T(1024)S(1)}, f32[2048]{0:T(1024)}, u32[]{:S(2)}) copy-start(f32[2048]{0:T(1024)} %param.29) | copy-start | bytes 24580
  6.5 104.3 %all-gather.7.cloned.1.call-start = ((), (), s32[]{:S(2)}) async-start(), calls=%async_computation.1 | async-start | bytes 2228224 | tf_op jit(solution)/shard_map/all_gather | solution.py:170
  10.2 6.0 %copy-start.4 = (bf16[2048,512]{1,0:T(8,128)(2,1)S(1)}, bf16[2048,512]{1,0:T(8,128)(2,1)}, u32[]{:S(2)}) copy-start(bf16[2048,512]{1,0:T(8,128)(2,1)} %param.32) | copy-start | bytes 6291460
  13.0 4.8 %copy-start.9 = (bf16[2048,256]{1,0:T(8,128)(2,1)S(1)}, bf16[2048,256]{1,0:T(8,128)(2,1)}, u32[]{:S(2)}) copy-start(bf16[2048,256]{1,0:T(8,128)(2,1)} %param.37) | copy-start | bytes 3145732
  16.2 2.6 copy-start.10
  16.2 3.7 %copy-start.5 = (bf16[2048,512]{1,0:T(8,128)(2,1)S(1)}, bf16[2048,512]{1,0:T(8,128)(2,1)}, u32[]{:S(2)}) copy-start(bf16[2048,512]{1,0:T(8,128)(2,1)} %param.39) | copy-start | bytes 6291460
  17.8 3.8 %copy-start.6 = (bf16[2048,512]{1,0:T(8,128)(2,1)S(1)}, bf16[2048,512]{1,0:T(8,128)(2,1)}, u32[]{:S(2)}) copy-start(bf16[2048,512]{1,0:T(8,128)(2,1)} %param.40) | copy-start | bytes 6291460
  23.9 8.4 %copy-start.16 = (f32[64]{0:T(128)S(1)}, f32[64]{0:T(128)}, u32[]{:S(2)}) copy-start(f32[64]{0:T(128)} %param.34) | copy-start | bytes 772
  23.9 13.8 %copy-start.20 = (bf16[32,256]{1,0:T(8,128)(2,1)S(1)}, bf16[32,256]{1,0:T(8,128)(2,1)}, u32[]{:S(2)}) copy-start(bf16[32,256]{1,0:T(8,128)(2,1)} %param.42) | copy-start | bytes 49156
  23.9 13.9 %copy-start.21 = (f32[256]{0:T(256)S(1)}, f32[256]{0:T(256)}, u32[]{:S(2)}) copy-start(f32[256]{0:T(256)} %param.43) | copy-start | bytes 3076
  32.2 7.6 %copy-start.14 = (f32[128,4]{0,1:T(4,128)S(1)}, f32[128,4]{0,1:T(4,128)}, u32[]{:S(2)}) copy-start(f32[128,4]{0,1:T(4,128)} %param.44) | copy-start | bytes 6148
  33.3 130.5 %all-gather.9.cloned.1.call-start = ((), (), s32[]{:S(2)}) async-start(), calls=%async_computation.2 | async-start | bytes 2228224 | tf_op jit(solution)/shard_map/all_gather | solution.py:171
  34.1 191.3 %all-gather.11.cloned.1.call-start = ((), (), s32[]{:S(2)}) async-start(), calls=%async_computation.4 | async-start | bytes 2228224 | tf_op jit(solution)/shard_map/all_gather | solution.py:31
  43.7 11.4 %copy-start.17 = (f32[64]{0:T(128)S(1)}, f32[64]{0:T(128)}, u32[]{:S(2)}) copy-start(f32[64]{0:T(128)} %param.33) | copy-start | bytes 772
  54.2 0.6 copy-start.3
  54.9 212.2 %reduce-scatter.2.cloned.1.call-start = ((), (), s32[]{:S(2)}) async-start(), calls=%async_computation.3 | async-start | bytes 786432 | tf_op jit(solution)/shard_map/reduce_scatter | solution.py:283
  55.6 5.3 %collective-permute-start = (bf16[64,512]{1,0:T(8,128)(2,1)S(1)}, bf16[64,512]{1,0:T(8,128)(2,1)S(1)}, u32[]{:S(2)}, u32[]{:S(2)}) collective-permute-start(bf16[64,512]{1,0:T(8,128)(2,1)S(1)} %reshape.212), channel_id=1, source_target_pairs={{0,2},{2,0},{4,6},{6,4},{8,10},{10,8},{12,14},{14,12},{16,18},{18,... | collective-permute-start | bytes 196616 | tf_op jit(solution)/shard_map/ppermute | solution.py:26
  60.9 45.7 %collective-permute-start.1 = (bf16[64,512]{1,0:T(8,128)(2,1)S(1)}, bf16[64,512]{1,0:T(8,128)(2,1)S(1)}, u32[]{:S(2)}, u32[]{:S(2)}) collective-permute-start(bf16[64,512]{1,0:T(8,128)(2,1)S(1)} %collective-permute-done), channel_id=1, source_target_pairs={{0,4},{4,0},{2,6},{6,2},{8,12},{12,8},{10,14},{14,10},{16,20},{20,... | collective-permute-start | bytes 196616 | tf_op jit(solution)/shard_map/ppermute | solution.py:26
  106.6 4.3 %collective-permute-start.2 = (bf16[64,512]{1,0:T(8,128)(2,1)S(1)}, bf16[64,512]{1,0:T(8,128)(2,1)S(1)}, u32[]{:S(2)}, u32[]{:S(2)}) collective-permute-start(bf16[64,512]{1,0:T(8,128)(2,1)S(1)} %collective-permute-done.1), channel_id=1, source_target_pairs={{0,8},{8,0},{2,10},{10,2},{4,12},{12,4},{6,14},{14,6},{16,24},{24,... | collective-permute-start | bytes 196616 | tf_op jit(solution)/shard_map/ppermute | solution.py:26
  110.9 53.0 %collective-permute-start.3 = (bf16[64,512]{1,0:T(8,128)(2,1)S(1)}, bf16[64,512]{1,0:T(8,128)(2,1)S(1)}, u32[]{:S(2)}, u32[]{:S(2)}) collective-permute-start(bf16[64,512]{1,0:T(8,128)(2,1)S(1)} %collective-permute-done.2), channel_id=1, source_target_pairs={{0,16},{16,0},{2,18},{18,2},{4,20},{20,4},{6,22},{22,6},{8,24},{24... | collective-permute-start | bytes 196616 | tf_op jit(solution)/shard_map/ppermute | solution.py:26
  166.9 1.6 copy-start.1
  169.4 5.7 %copy-start.15 = (f32[4]{0:T(128)S(1)}, f32[4]{0:T(128)}, u32[]{:S(2)}) copy-start(f32[4]{0:T(128)} %param.35) | copy-start | bytes 52
  169.4 6.2 %copy-start.18 = (f32[128]{0:T(128)S(1)}, f32[128]{0:T(128)}, u32[]{:S(2)}) copy-start(f32[128]{0:T(128)} %param.36) | copy-start | bytes 1540
  172.2 1.6 copy-start.2
  174.7 75.5 %copy-start.11 = (f32[128,512]{0,1:T(8,128)S(1)}, f32[128,512]{0,1:T(8,128)}, u32[]{:S(2)}) copy-start(f32[128,512]{0,1:T(8,128)} %get-tuple-element.532) | copy-start | bytes 786436
  174.7 75.5 %copy-start.19 = (f32[128]{0:T(128)S(1)}, f32[128]{0:T(128)}, u32[]{:S(2)}) copy-start(f32[128]{0:T(128)} %param.45) | copy-start | bytes 1540
  176.0 68.4 %collective-permute-start.4 = (bf16[64,512]{1,0:T(8,128)(2,1)S(1)}, bf16[64,512]{1,0:T(8,128)(2,1)S(1)}, u32[]{:S(2)}, u32[]{:S(2)}) collective-permute-start(bf16[64,512]{1,0:T(8,128)(2,1)S(1)} %bitcast.194), channel_id=1, source_target_pairs={{0,2},{2,0},{4,6},{6,4},{8,10},{10,8},{12,14},{14,12},{16,18},{18,... | collective-permute-start | bytes 196616 | tf_op jit(solution)/shard_map/ppermute | solution.py:26
  242.6 15.5 %copy-start.7 = (bf16[512,2048]{1,0:T(8,128)(2,1)S(1)}, bf16[512,2048]{1,0:T(8,128)(2,1)}, u32[]{:S(2)}) copy-start(bf16[512,2048]{1,0:T(8,128)(2,1)} %param.46) | copy-start | bytes 6291460
  244.4 4.3 %collective-permute-start.5 = (bf16[64,512]{1,0:T(8,128)(2,1)S(1)}, bf16[64,512]{1,0:T(8,128)(2,1)S(1)}, u32[]{:S(2)}, u32[]{:S(2)}) collective-permute-start(bf16[64,512]{1,0:T(8,128)(2,1)S(1)} %collective-permute-done.4), channel_id=1, source_target_pairs={{0,4},{4,0},{2,6},{6,2},{8,12},{12,8},{10,14},{14,10},{16,20},{20,... | collective-permute-start | bytes 196616 | tf_op jit(solution)/shard_map/ppermute | solution.py:26
  248.7 4.3 %collective-permute-start.6 = (bf16[64,512]{1,0:T(8,128)(2,1)S(1)}, bf16[64,512]{1,0:T(8,128)(2,1)S(1)}, u32[]{:S(2)}, u32[]{:S(2)}) collective-permute-start(bf16[64,512]{1,0:T(8,128)(2,1)S(1)} %collective-permute-done.5), channel_id=1, source_target_pairs={{0,8},{8,0},{2,10},{10,2},{4,12},{12,4},{6,14},{14,6},{16,24},{24,... | collective-permute-start | bytes 196616 | tf_op jit(solution)/shard_map/ppermute | solution.py:26
  253.0 5.2 %collective-permute-start.7 = (bf16[64,512]{1,0:T(8,128)(2,1)S(1)}, bf16[64,512]{1,0:T(8,128)(2,1)S(1)}, u32[]{:S(2)}, u32[]{:S(2)}) collective-permute-start(bf16[64,512]{1,0:T(8,128)(2,1)S(1)} %collective-permute-done.6), channel_id=1, source_target_pairs={{0,16},{16,0},{2,18},{18,2},{4,20},{20,4},{6,22},{22,6},{8,24},{24... | collective-permute-start | bytes 196616 | tf_op jit(solution)/shard_map/ppermute | solution.py:26
Sparse Core Ops, SparseCore 0:
  33.4 65.8 all-gather.6
  102.0 61.7 all-gather.8
  166.6 58.7 all-gather.10
  259.6 7.4 reduce-scatter.1
where the time goes:
time: 274 us
  waiting for transfers between devices  124 us (45%)
  blocking collectives  43.2 us (16%)
  other arithmetic  29.7 us (11%)
  local copies, waits for them, and re-layouts  27 us (10%)
  matrix products  23 us (8%)
  between operations  14.8 us (5%)
  starting transfers between devices  11.2 us (4%)
    all_gather x1, waiting for transfers between devices, per_device(): value_rows = lax.all_gather(value_flat, 'sp', axis=0, tiled=True)  52.9 us
    all_gather x1, waiting for transfers between devices, prefix(): everything = jax.tree.map(lambda part: lax.all_gather(part, axis), shard)  47.9 us
    all_gather x1, blocking collectives, prefix(): everything = jax.tree.map(lambda part: lax.all_gather(part, axis), shard)  40.7 us
    select_n x16, other arithmetic, turn(): return jax.tree.map(lambda a, b: jnp.where(reached, a, b), new, before)  16.6 us
    unnamed x52, local copies, waits for them, and re-layouts  15.6 us
    ppermute x8, waiting for transfers between devices, partner(): return lax.ppermute(block, axis, route)  15 us
    ppermute x8, starting transfers between devices, partner(): return lax.ppermute(block, axis, route)  11.1 us
    dot_general x1, matrix products, per_device(): jnp.dot(lax.all_gather(normed, 'tp', axis=0, tiled=True), packed, preferr...  8.26 us
  transfers between devices with their start and end apart: 12, of which 8 were waited for; matrix products, arithmetic and copies ran while one was open for 19% of the time, Pallas kernels for 0%

commit v1 on v0

--- a/solution.py
+++ b/solution.py
@@ -168,7 +168,9 @@
         )
     )
     key_rows = lax.all_gather(key_flat, "sp", axis=0, tiled=True)
-    value_rows = lax.all_gather(value_flat, "sp", axis=0, tiled=True)
+    value_rows = jnp.concatenate(
+        lax.all_to_all(jnp.stack([value_flat] * lax.axis_size("sp")), "sp", 0, 0), axis=0
+    )
     piece_rows = key_rows.shape[0]
     span_rows = block_length(piece_rows, row_count)
 

time: 274 us -> 231 us (0.84)
  waiting for transfers between devices: 124 us -> 54.4 us
  starting transfers between devices: 11.2 us -> 28.3 us
  local copies, waits for them, and re-layouts: 27 us -> 37.2 us
    all_gather x1 -> x0, waiting for transfers between devices: 52.9 us -> none  [per_device(): value_rows = lax.all_gather(value_flat, 'sp', axis=0, tiled=True)]
    all_gather x1, waiting for transfers between devices: 47.9 us -> 29 us  [prefix(): everything = jax.tree.map(lambda part: lax.all_gather(part, axis), shard)]
    ppermute x8, starting transfers between devices: 11.1 us -> 20 us  [partner(): return lax.ppermute(block, axis, route)]
    all_to_all x0 -> x1, starting transfers between devices: none -> 8.27 us  [per_device(): lax.all_to_all(jnp.stack([value_flat] * lax.axis_size('sp')), 'sp', 0, 0)]
    all_to_all x0 -> x1, local copies, waits for them, and re-layouts: none -> 4.28 us  [per_device(): lax.all_to_all(jnp.stack([value_flat] * lax.axis_size('sp')), 'sp', 0, 0)]
    reshape x0 -> x1, local copies, waits for them, and re-layouts: none -> 4.15 us  [attend(): values_here = lax.dynamic_slice_in_dim(value_rows, span_index * span_rows...]
  transfers between devices with their start and end apart: 12 -> 12, of which waited for: 8 -> 7; matrix products, arithmetic and copies ran while one was open for 19% -> 27% of each run, Pallas kernels for 0% -> 0%
where the time goes in v1:
time: 231 us; the launch traced here: 230 us
  waiting for transfers between devices  54.4 us (24%)
  blocking collectives  42.4 us (18%)
  local copies, waits for them, and re-layouts  37.2 us (16%)
  other arithmetic  29.1 us (13%)
  starting transfers between devices  28.3 us (12%)
  matrix products  23.2 us (10%)
  between operations  14.8 us (6%)
    all_gather x1, blocking collectives, prefix(): everything = jax.tree.map(lambda part: lax.all_gather(part, axis), shard)  40 us
    all_gather x1, waiting for transfers between devices, prefix(): everything = jax.tree.map(lambda part: lax.all_gather(part, axis), shard)  29 us
    ppermute x8, starting transfers between devices, partner(): return lax.ppermute(block, axis, route)  20 us
    ppermute x8, waiting for transfers between devices, partner(): return lax.ppermute(block, axis, route)  17.8 us
    select_n x16, other arithmetic, turn(): return jax.tree.map(lambda a, b: jnp.where(reached, a, b), new, before)  16.6 us
    unnamed x52, local copies, waits for them, and re-layouts  15.7 us
    all_to_all x1, starting transfers between devices, per_device(): lax.all_to_all(jnp.stack([value_flat] * lax.axis_size('sp')), 'sp', 0, 0)  8.27 us
    dot_general x1, matrix products, per_device(): jnp.dot(lax.all_gather(normed, 'tp', axis=0, tiled=True), packed, preferr...  8.23 us
  transfers between devices with their start and end apart: 12, of which 7 were waited for; matrix products, arithmetic and copies ran while one was open for 27% of the time, Pallas kernels for 0%

profile of v1, /device:TPU:0, one launch (start us, length us, event | category | flops | bytes accessed | tf_op | source)
XLA Modules:
  0.0 230.4 jit_solution(5085075636794993614)
XLA Ops:
  6.6 3.4 %constant_dynamic-update-slice_fusion.7 = bf16[2048,3104]{1,0:T(8,128)(2,1)} fusion(bf16[2048,512]{1,0:T(8,128)(2,1)} %param.30), kind=kLoop, calls=%fused_computation.130 | loop fusion | bytes 4194304
  10.6 2.4 %all_gather.18 = bf16[128,2048]{1,0:T(8,128)(2,1)S(1)} all-gather(bf16[64,2048]{1,0:T(8,128)(2,1)S(1)} %fusion.46), channel_id=1, replica_groups=mesh['sp'=16,'tp'=2] {'tp'}, dimensions={0}, use_global_device_ids=true | all-gather | bytes 786432 | tf_op jit(solution)/shard_map/all_gather | solution.py:132
  13.0 3.2 %constant_dynamic-update-slice_fusion.6 = bf16[2048,3104]{1,0:T(8,128)(2,1)} fusion(bf16[2048,3104]{1,0:T(8,128)(2,1)} %constant_dynamic-update-slice_fusion.7, bf16[2048,512]{1,0:T(8,128)(2,1)} %param.31), kind=kLoop, calls=%fused_computation.129 | loop fusion | bytes 4194304
  16.2 1.6 constant_dynamic-update-slice_fusion.5
  17.8 1.1 constant_dynamic-update-slice_fusion.4
  18.9 1.1 constant_dynamic-update-slice_fusion.3
  20.0 1.5 constant_dynamic-update-slice_fusion.2
  21.6 1.5 constant_dynamic-update-slice_fusion.1
  24.0 8.2 %convolution_convert_fusion = bf16[128,3104]{0,1:T(8,128)(2,1)S(1)} fusion(bf16[128,2048]{1,0:T(8,128)(2,1)S(1)} %all_gather.18, bf16[2048,3104]{1,0:T(8,128)(2,1)} %constant_dynamic-update-slice_fusion), kind=kOutput, calls=%fused_computation.68 | convolution fusion | flops 1627787264 | bytes 14032896 | tf_op jit(solution)/shard_map/dot_general | solution.py:131
  33.4 1.7 stack.2
  35.1 8.3 %all-to-all-start = ((bf16[16,128,512]{1,2,0:T(8,128)(2,1)}), bf16[16,128,512]{1,2,0:T(8,128)(2,1)}, u32[]{:S(2)}, u32[]{:S(2)}) async-start(bf16[16,128,512]{1,2,0:T(8,128)(2,1)} %stack.2), calls=%async_computation | async-start | bytes 4194304 | tf_op jit(solution)/shard_map/all_to_all | solution.py:172
  44.8 1.1 reshape.232
  45.9 1.2 copy.127
  48.1 1.1 div.64
  49.3 1.1 mul.296
  50.4 1.8 reshape.223
  53.1 10.5 %while.8 = (s32[]{:T(128)}, f32[4,64,128]{2,1,0:T(8,128)S(1)}, f32[4,64]{1,0:T(4,128)S(1)}, f32[2,64,4,128]{3,1,0,2:T(8,128)}, f32[2,64,4,64]{3,2,1,0:T(4,128)},...) while((s32[]{:T(128)}, f32[4,64,128]{2,1,0:T(8,128)S(1)}, ...), condition=%wide.region_17.18_spmd.clone, body=%wide.region_15.0_spmd.clone.sunk | while | flops 89412096 | bytes 2970753 | solution.py:258
  53.1 1.2 constant_dynamic-slice_fusion.3
  58.3 1.2 constant_dynamic-slice_fusion.3
  64.9 1.9 collective-permute-start
  66.9 7.1 %collective-permute-done = bf16[64,512]{1,0:T(8,128)(2,1)S(1)} collective-permute-done((bf16[64,512]{1,0:T(8,128)(2,1)S(1)}, bf16[64,512]{1,0:T(8,128)(2,1)S(1)}, u32[]{:S(2)}, u32[]{:S(2)}) %collective-permute-start) | collective-permute-done | bytes 65568 | tf_op jit(solution)/shard_map/ppermute | solution.py:26
  76.0 1.1 copy.131
  77.1 40.0 %all-gather.2 = f32[16,4,64]{2,1,0:T(4,128)S(1)} all-gather(f32[1,4,64]{2,1,0:T(4,128)S(1)} %exponential_bitcast_fusion), channel_id=2, replica_groups=mesh['sp'=16,'tp'=2] {'sp'}, dimensions={0}, use_global_device_ids=true | all-gather | bytes 17408 | tf_op jit(solution)/shard_map/all_gather | solution.py:31
  117.1 7.9 %collective-permute-start.2 = (bf16[64,512]{1,0:T(8,128)(2,1)S(1)}, bf16[64,512]{1,0:T(8,128)(2,1)S(1)}, u32[]{:S(2)}, u32[]{:S(2)}) collective-permute-start(bf16[64,512]{1,0:T(8,128)(2,1)S(1)} %collective-permute-done.1), channel_id=1, source_target_pairs={{0,8},{8,0},{2,10},{10,2},{4,12},{12,4},{6,14},{14,6},{16,24},{24,... | collective-permute-start | bytes 196616 | tf_op jit(solution)/shard_map/ppermute | solution.py:26
  125.0 2.2 collective-permute-done.2
  127.3 4.6 %collective-permute-start.3 = (bf16[64,512]{1,0:T(8,128)(2,1)S(1)}, bf16[64,512]{1,0:T(8,128)(2,1)S(1)}, u32[]{:S(2)}, u32[]{:S(2)}) collective-permute-start(bf16[64,512]{1,0:T(8,128)(2,1)S(1)} %collective-permute-done.2), channel_id=1, source_target_pairs={{0,16},{16,0},{2,18},{18,2},{4,20},{20,4},{6,22},{22,6},{8,24},{24... | collective-permute-start | bytes 196616 | tf_op jit(solution)/shard_map/ppermute | solution.py:26
  131.8 4.3 %copy.112 = bf16[16,128,512]{1,0,2:T(8,128)(2,1)} copy(bf16[16,128,512]{1,2,0:T(8,128)(2,1)} %all-to-all-done) | data formatting | bytes 4194304 | tf_op jit(solution)/shard_map/all_to_all | solution.py:172
  136.1 4.2 %reshape.214 = bf16[2048,4,128]{0,2,1:T(8,128)(2,1)} reshape(bf16[16,128,512]{1,0,2:T(8,128)(2,1)} %copy.112) | data formatting | bytes 4194304 | tf_op jit(solution)/shard_map/while/body/eval_jaxpr/reshape | solution.py:184
  140.3 5.5 %conditional.3 = (f32[8,64]{1,0:T(8,128)S(1)}, f32[8,64,128]{2,1,0:T(8,128)S(1)}) conditional(s32[]{:T(128)} %convert_element_type.81, (f32[8,64]{1,0:T(8,128)S(1)}, f32[8,64,128]{2,1,0:T(8,128)S(1)}) %tuple.49, (s32[2048]{0:T(1024)S(1)}, s32[64]{0:T(128)S(1)}, bf16[64,512]{1,0:T(8,128)(2,1)S(1)}, bf16[2048,8,64]{0,2,1:T(8,128)(2,1)}, ...), branch_computations={%region_10.0_spmd, %region_11.0_spmd} | conditional | flops 412353536 | bytes 26839340 | solution.py:189
  140.8 2.6 %fusion.9 = (f32[8,64]{1,0:T(8,128)S(1)}, f32[8,64,2048]{2,1,0:T(8,128)S(1)}) fusion(pred[64,2048]{1,0:T(8,128)(4,1)S(1)} %broadcast_compare_fusion.1, bf16[2048,8,64]{0,2,1:T(8,128)(2,1)} %get-tuple-element.263, bf16[64,8,64]{2,1,0:T(8,128)(2,1)S(1)} %reshape.198), kind=kOutput, calls=%fused_computation.16 | convolution fusion | flops 137362944 | bytes 6490112 | tf_op jit(solution)/shard_map/while/body/eval_jaxpr/cond/branch_1_fun/tgd,kgd->gtk/dot_general | solution.py:74
  143.4 1.3 fusion.10
  145.9 5.4 %conditional.2 = ((f32[8,64]{1,0:T(8,128)S(1)}, f32[8,64,128]{2,1,0:T(8,128)S(1)})) conditional(s32[]{:T(128)} %convert_element_type.71, (f32[8,64]{1,0:T(8,128)S(1)}, f32[8,64,128]{2,1,0:T(8,128)S(1)}) %tuple.49, (s32[2048]{0:T(1024)S(1)}, s32[64]{0:T(128)S(1)}, bf16[128,8,64]{2,0,1:T(8,128)(2,1)S(1)}, bf16[2048,8,64]{0,2,1:T(8,128)(2,1)}, ...), branch_computations={%region_4.5_spmd, %region_5.8_spmd} | conditional | flops 412353536 | bytes 26773812 | solution.py:189
  146.0 2.7 %fusion.2 = (f32[8,64]{1,0:T(8,128)S(1)}, f32[8,64,2048]{2,1,0:T(8,128)S(1)}) fusion(pred[64,2048]{1,0:T(8,128)(4,1)S(1)} %broadcast_compare_fusion, bf16[2048,8,64]{0,2,1:T(8,128)(2,1)} %get-tuple-element.255, bf16[128,8,64]{2,0,1:T(8,128)(2,1)S(1)} %get-tuple-element.254), kind=kOutput, calls=%fused_computation.3 | convolution fusion | flops 137362944 | bytes 6555648 | tf_op jit(solution)/shard_map/while/body/eval_jaxpr/cond/branch_1_fun/tgd,kgd->gtk/dot_general | solution.py:74
  148.8 1.3 fusion.3
  153.2 29.0 %all-gather.8.cloned.1.call-done = f32[64,64,128]{2,1,0:T(8,128)} async-done(((f32[4,64,128]{2,1,0:T(8,128)}), f32[64,64,128]{2,1,0:T(8,128)}) %all-gather.8.cloned.1.call-update) | async-done | bytes 2097168 | tf_op jit(solution)/shard_map/all_gather | solution.py:31
  182.2 17.2 %while.9 = (s32[]{:T(128)}, f32[4,64,128]{2,1,0:T(8,128)S(1)}, s32[]{:T(128)}, f32[16,4,64]{2,1,0:T(4,128)S(1)}, f32[16,4,64,128]{3,2,1,0:T(8,128)}, /*index=5*/s32[]{:T(128)}, s32[]{:T(128)}) while((s32[]{:T(128)}, f32[4,64,128]{2,1,0:T(8,128)S(1)}, s32[]{:T(128)}, f32[16,4,64]{2,1,0:T(4,128)S(1)}, ...), condition=%wide.region_19.20_spmd.clone, body=%wide.region_18.19_spmd.clone.sunk | while | flops 131076 | bytes 396393 | solution.py:43
  183.3 1.0 fusion.107
  184.4 1.0 fusion.107
  185.5 1.0 fusion.107
  199.5 1.7 multiply_reduce_fusion
  201.2 1.5 collective-permute-start.5
  202.8 2.8 %collective-permute-done.5 = bf16[64,512]{1,0:T(8,128)(2,1)S(1)} collective-permute-done((bf16[64,512]{1,0:T(8,128)(2,1)S(1)}, bf16[64,512]{1,0:T(8,128)(2,1)S(1)}, u32[]{:S(2)}, u32[]{:S(2)}) %collective-permute-start.5) | collective-permute-done | bytes 65568 | tf_op jit(solution)/shard_map/ppermute | solution.py:26
  205.6 1.5 collective-permute-start.6
  207.1 2.7 %collective-permute-done.6 = bf16[64,512]{1,0:T(8,128)(2,1)S(1)} collective-permute-done((bf16[64,512]{1,0:T(8,128)(2,1)S(1)}, bf16[64,512]{1,0:T(8,128)(2,1)S(1)}, u32[]{:S(2)}, u32[]{:S(2)}) %collective-permute-start.6) | collective-permute-done | bytes 65568 | tf_op jit(solution)/shard_map/ppermute | solution.py:26
  209.8 1.8 collective-permute-start.7
  212.1 2.9 %collective-permute-done.7 = bf16[64,512]{1,0:T(8,128)(2,1)S(1)} collective-permute-done((bf16[64,512]{1,0:T(8,128)(2,1)S(1)}, bf16[64,512]{1,0:T(8,128)(2,1)S(1)}, u32[]{:S(2)}, u32[]{:S(2)}) %collective-permute-start.7) | collective-permute-done | bytes 65568 | tf_op jit(solution)/shard_map/ppermute | solution.py:26
  215.0 1.3 fusion.41
  216.3 7.6 %reduce-scatter.2.cloned.1.call-done = bf16[64,2048]{1,0:T(8,128)(2,1)} async-done(((bf16[128,2048]{1,0:T(8,128)(2,1)}), bf16[64,2048]{1,0:T(8,128)(2,1)}) %reduce-scatter.2.cloned.1.call-update) | async-done | bytes 262160 | tf_op jit(solution)/shard_map/reduce_scatter | solution.py:285
  (170 shorter events, 34.7 us)
Async XLA Ops:
  6.5 205.1 %copy-start = (bf16[512,2048]{1,0:T(8,128)(2,1)S(1)}, bf16[512,2048]{1,0:T(8,128)(2,1)}, u32[]{:S(2)}) copy-start(bf16[512,2048]{1,0:T(8,128)(2,1)} %param.47) | copy-start | bytes 6291460
  6.5 3.4 %copy-start.12 = (bf16[2048,32]{0,1:T(8,128)(2,1)S(1)}, bf16[2048,32]{0,1:T(8,128)(2,1)}, u32[]{:S(2)}) copy-start(bf16[2048,32]{0,1:T(8,128)(2,1)} %param.41) | copy-start | bytes 393220
  6.5 3.7 %copy-start.8 = (bf16[64,2048]{1,0:T(8,128)(2,1)S(1)}, bf16[64,2048]{1,0:T(8,128)(2,1)}, u32[]{:S(2)}) copy-start(bf16[64,2048]{1,0:T(8,128)(2,1)} %param.28) | copy-start | bytes 786436
  6.5 3.9 %copy-start.13 = (f32[2048]{0:T(1024)S(1)}, f32[2048]{0:T(1024)}, u32[]{:S(2)}) copy-start(f32[2048]{0:T(1024)} %param.29) | copy-start | bytes 24580
  6.5 133.7 %all-gather.6.cloned.1.call-start = ((), (), s32[]{:S(2)}) async-start(), calls=%async_computation.2 | async-start | bytes 2228224 | tf_op jit(solution)/shard_map/all_gather | solution.py:170
  10.2 6.0 %copy-start.4 = (bf16[2048,512]{1,0:T(8,128)(2,1)S(1)}, bf16[2048,512]{1,0:T(8,128)(2,1)}, u32[]{:S(2)}) copy-start(bf16[2048,512]{1,0:T(8,128)(2,1)} %param.32) | copy-start | bytes 6291460
  13.0 4.8 %copy-start.9 = (bf16[2048,256]{1,0:T(8,128)(2,1)S(1)}, bf16[2048,256]{1,0:T(8,128)(2,1)}, u32[]{:S(2)}) copy-start(bf16[2048,256]{1,0:T(8,128)(2,1)} %param.37) | copy-start | bytes 3145732
  16.2 2.7 %copy-start.10 = (bf16[2048,256]{1,0:T(8,128)(2,1)S(1)}, bf16[2048,256]{1,0:T(8,128)(2,1)}, u32[]{:S(2)}) copy-start(bf16[2048,256]{1,0:T(8,128)(2,1)} %param.38) | copy-start | bytes 3145732
  16.2 3.8 %copy-start.5 = (bf16[2048,512]{1,0:T(8,128)(2,1)S(1)}, bf16[2048,512]{1,0:T(8,128)(2,1)}, u32[]{:S(2)}) copy-start(bf16[2048,512]{1,0:T(8,128)(2,1)} %param.39) | copy-start | bytes 6291460
  17.8 3.8 %copy-start.6 = (bf16[2048,512]{1,0:T(8,128)(2,1)S(1)}, bf16[2048,512]{1,0:T(8,128)(2,1)}, u32[]{:S(2)}) copy-start(bf16[2048,512]{1,0:T(8,128)(2,1)} %param.40) | copy-start | bytes 6291460
  24.0 8.3 %copy-start.16 = (f32[64]{0:T(128)S(1)}, f32[64]{0:T(128)}, u32[]{:S(2)}) copy-start(f32[64]{0:T(128)} %param.34) | copy-start | bytes 772
  33.3 13.8 %copy-start.20 = (bf16[32,256]{1,0:T(8,128)(2,1)S(1)}, bf16[32,256]{1,0:T(8,128)(2,1)}, u32[]{:S(2)}) copy-start(bf16[32,256]{1,0:T(8,128)(2,1)} %param.42) | copy-start | bytes 49156
  33.3 13.8 %copy-start.21 = (f32[256]{0:T(256)S(1)}, f32[256]{0:T(256)}, u32[]{:S(2)}) copy-start(f32[256]{0:T(256)} %param.43) | copy-start | bytes 3076
  33.4 15.8 %copy-start.14 = (f32[128,4]{0,1:T(4,128)S(1)}, f32[128,4]{0,1:T(4,128)}, u32[]{:S(2)}) copy-start(f32[128,4]{0,1:T(4,128)} %param.44) | copy-start | bytes 6148
  35.1 96.7 %all-to-all-start = ((bf16[16,128,512]{1,2,0:T(8,128)(2,1)}), bf16[16,128,512]{1,2,0:T(8,128)(2,1)}, u32[]{:S(2)}, u32[]{:S(2)}) async-start(bf16[16,128,512]{1,2,0:T(8,128)(2,1)} %stack.2), calls=%async_computation | async-start | bytes 4194304 | tf_op jit(solution)/shard_map/all_to_all | solution.py:172
  43.4 138.8 %all-gather.8.cloned.1.call-start = ((), (), s32[]{:S(2)}) async-start(), calls=%async_computation.4 | async-start | bytes 2228224 | tf_op jit(solution)/shard_map/all_gather | solution.py:31
  53.1 11.4 %copy-start.17 = (f32[64]{0:T(128)S(1)}, f32[64]{0:T(128)}, u32[]{:S(2)}) copy-start(f32[64]{0:T(128)} %param.33) | copy-start | bytes 772
  63.6 0.7 copy-start.3
  64.3 159.6 %reduce-scatter.2.cloned.1.call-start = ((), (), s32[]{:S(2)}) async-start(), calls=%async_computation.3 | async-start | bytes 786432 | tf_op jit(solution)/shard_map/reduce_scatter | solution.py:285
  64.9 9.1 %collective-permute-start = (bf16[64,512]{1,0:T(8,128)(2,1)S(1)}, bf16[64,512]{1,0:T(8,128)(2,1)S(1)}, u32[]{:S(2)}, u32[]{:S(2)}) collective-permute-start(bf16[64,512]{1,0:T(8,128)(2,1)S(1)} %reshape.216), channel_id=1, source_target_pairs={{0,2},{2,0},{4,6},{6,4},{8,10},{10,8},{12,14},{14,12},{16,18},{18,... | collective-permute-start | bytes 196616 | tf_op jit(solution)/shard_map/ppermute | solution.py:26
  74.0 43.0 %collective-permute-start.1 = (bf16[64,512]{1,0:T(8,128)(2,1)S(1)}, bf16[64,512]{1,0:T(8,128)(2,1)S(1)}, u32[]{:S(2)}, u32[]{:S(2)}) collective-permute-start(bf16[64,512]{1,0:T(8,128)(2,1)S(1)} %collective-permute-done), channel_id=1, source_target_pairs={{0,4},{4,0},{2,6},{6,2},{8,12},{12,8},{10,14},{14,10},{16,20},{20,... | collective-permute-start | bytes 196616 | tf_op jit(solution)/shard_map/ppermute | solution.py:26
  117.1 10.2 %collective-permute-start.2 = (bf16[64,512]{1,0:T(8,128)(2,1)S(1)}, bf16[64,512]{1,0:T(8,128)(2,1)S(1)}, u32[]{:S(2)}, u32[]{:S(2)}) collective-permute-start(bf16[64,512]{1,0:T(8,128)(2,1)S(1)} %collective-permute-done.1), channel_id=1, source_target_pairs={{0,8},{8,0},{2,10},{10,2},{4,12},{12,4},{6,14},{14,6},{16,24},{24,... | collective-permute-start | bytes 196616 | tf_op jit(solution)/shard_map/ppermute | solution.py:26
  127.3 13.0 %collective-permute-start.3 = (bf16[64,512]{1,0:T(8,128)(2,1)S(1)}, bf16[64,512]{1,0:T(8,128)(2,1)S(1)}, u32[]{:S(2)}, u32[]{:S(2)}) collective-permute-start(bf16[64,512]{1,0:T(8,128)(2,1)S(1)} %collective-permute-done.2), channel_id=1, source_target_pairs={{0,16},{16,0},{2,18},{18,2},{4,20},{20,4},{6,22},{22,6},{8,24},{24... | collective-permute-start | bytes 196616 | tf_op jit(solution)/shard_map/ppermute | solution.py:26
  143.4 1.6 copy-start.1
  145.8 5.8 %copy-start.15 = (f32[4]{0:T(128)S(1)}, f32[4]{0:T(128)}, u32[]{:S(2)}) copy-start(f32[4]{0:T(128)} %param.35) | copy-start | bytes 52
  145.8 6.2 %copy-start.18 = (f32[128]{0:T(128)S(1)}, f32[128]{0:T(128)}, u32[]{:S(2)}) copy-start(f32[128]{0:T(128)} %param.36) | copy-start | bytes 1540
  148.8 1.6 copy-start.2
  151.2 55.8 %copy-start.11 = (f32[128,512]{0,1:T(8,128)S(1)}, f32[128,512]{0,1:T(8,128)}, u32[]{:S(2)}) copy-start(f32[128,512]{0,1:T(8,128)} %get-tuple-element.516) | copy-start | bytes 786436
  151.2 55.8 %copy-start.19 = (f32[128]{0:T(128)S(1)}, f32[128]{0:T(128)}, u32[]{:S(2)}) copy-start(f32[128]{0:T(128)} %param.45) | copy-start | bytes 1540
  152.5 48.7 %collective-permute-start.4 = (bf16[64,512]{1,0:T(8,128)(2,1)S(1)}, bf16[64,512]{1,0:T(8,128)(2,1)S(1)}, u32[]{:S(2)}, u32[]{:S(2)}) collective-permute-start(bf16[64,512]{1,0:T(8,128)(2,1)S(1)} %bitcast.193), channel_id=1, source_target_pairs={{0,2},{2,0},{4,6},{6,4},{8,10},{10,8},{12,14},{14,12},{16,18},{18,... | collective-permute-start | bytes 196616 | tf_op jit(solution)/shard_map/ppermute | solution.py:26
  199.5 15.5 %copy-start.7 = (bf16[512,2048]{1,0:T(8,128)(2,1)S(1)}, bf16[512,2048]{1,0:T(8,128)(2,1)}, u32[]{:S(2)}) copy-start(bf16[512,2048]{1,0:T(8,128)(2,1)} %param.46) | copy-start | bytes 6291460
  201.2 4.3 %collective-permute-start.5 = (bf16[64,512]{1,0:T(8,128)(2,1)S(1)}, bf16[64,512]{1,0:T(8,128)(2,1)S(1)}, u32[]{:S(2)}, u32[]{:S(2)}) collective-permute-start(bf16[64,512]{1,0:T(8,128)(2,1)S(1)} %collective-permute-done.4), channel_id=1, source_target_pairs={{0,4},{4,0},{2,6},{6,2},{8,12},{12,8},{10,14},{14,10},{16,20},{20,... | collective-permute-start | bytes 196616 | tf_op jit(solution)/shard_map/ppermute | solution.py:26
  205.6 4.3 %collective-permute-start.6 = (bf16[64,512]{1,0:T(8,128)(2,1)S(1)}, bf16[64,512]{1,0:T(8,128)(2,1)S(1)}, u32[]{:S(2)}, u32[]{:S(2)}) collective-permute-start(bf16[64,512]{1,0:T(8,128)(2,1)S(1)} %collective-permute-done.5), channel_id=1, source_target_pairs={{0,8},{8,0},{2,10},{10,2},{4,12},{12,4},{6,14},{14,6},{16,24},{24,... | collective-permute-start | bytes 196616 | tf_op jit(solution)/shard_map/ppermute | solution.py:26
  209.8 5.2 %collective-permute-start.7 = (bf16[64,512]{1,0:T(8,128)(2,1)S(1)}, bf16[64,512]{1,0:T(8,128)(2,1)S(1)}, u32[]{:S(2)}, u32[]{:S(2)}) collective-permute-start(bf16[64,512]{1,0:T(8,128)(2,1)S(1)} %collective-permute-done.6), channel_id=1, source_target_pairs={{0,16},{16,0},{2,18},{18,2},{4,20},{20,4},{6,22},{22,6},{8,24},{24... | collective-permute-start | bytes 196616 | tf_op jit(solution)/shard_map/ppermute | solution.py:26
Sparse Core Ops, SparseCore 0:
  33.4 87.3 all-gather.5
  123.5 58.6 all-gather.7
  216.4 7.4 reduce-scatter.1
